TPU v7x, 256 devices: a whole 4x4x8 slice. The times are simulated.
256 devices in a mesh: sp: 32 (over z, x), tp: 8 (over y, core).
Axes of the slice: x: 4, y: 4, z: 8, core: 2. Of those that a mesh axis runs over, the one named last changes fastest.
Arguments:
- broad_probe_tensor: bfloat16 [16384, 1024], P('sp', 'tp'), may hold values from -6 to 6
- broad_lookup_tensor: bfloat16 [16384, 1024], P('sp', 'tp'), may hold values from -6 to 6
- broad_payload_tensor: bfloat16 [16384, 1024], P('sp', 'tp'), may hold values from -6 to 6
- broad_emission_valve: bfloat16 [16384, 1024], P('sp', 'tp'), may hold values from -6 to 6
- slim_probe_tensor: bfloat16 [16384, 1024], P('sp', 'tp'), may hold values from -6 to 6
- slim_lookup_tensor: bfloat16 [16384, 1024], P('sp', 'tp'), may hold values from -6 to 6
- slim_payload_tensor: bfloat16 [16384, 1024], P('sp', 'tp'), may hold values from -6 to 6
- slim_emission_valve: bfloat16 [16384, 1024], P('sp', 'tp'), may hold values from -6 to 6
- broad_forgetting_speed: float32 [8], P('tp'), may hold values from -0.08 to 0
- slim_forgetting_speed: float32 [16], P('tp'), may hold values from -0.08 to 0
- broad_channel_scaling: float32 [1024], P('tp'), may hold values from 0.1 to 1.9
- slim_channel_scaling: float32 [1024], P('tp'), may hold values from 0.1 to 1.9
- surge_forgetting: float32 [16384], P('sp'), may hold values from -2.1 to 0
- broad_emission_proj: bfloat16 [1024, 2048], replicated, may hold values from -0.125 to 0.125
- slim_emission_proj: bfloat16 [1024, 2048], replicated, may hold values from -0.125 to 0.125
- skip_stream: bfloat16 [16384, 2048], P(('sp', 'tp')), may hold values from -6 to 6
- premix_scaling_coeffs: float32 [2048], replicated, may hold values from 0.1 to 1.9
- routed_specialist_ids: int32 [16384, 2], P('sp'), may hold values from 0 to 31, as said below
- routed_specialist_shares: float32 [16384, 2], P('sp'), may hold values from 0.2 to 1
- specialist_valve_proj: bfloat16 [32, 2048, 2048], P('sp', None, 'tp'), may hold values from -0.125 to 0.125
- specialist_expand_proj: bfloat16 [32, 2048, 2048], P('sp', None, 'tp'), may hold values from -0.125 to 0.125
- specialist_contract_proj: bfloat16 [32, 2048, 2048], P('sp', 'tp'), may hold values from -0.125 to 0.125
Outputs:
- result: bfloat16 [16384, 2048], P(('sp', 'tp'))
Inputs may be any that keep to these rules, and one draw needn't show every extreme that they name: `routed_specialist_ids`: each row names two different experts of one group, that is of the same run of 8 consecutive experts. The rows of one device (each aligned block of 64 rows) name each expert at most 8 times, and some expert is named exactly 8 times by the rows of every device.
All inputs are finite; a program needn't handle non-finite values.
Results may differ from a plain program's by a relative error of at most 0.018.
Values may be sent and summed in bfloat16 or wider, within the bound.
A program may use at most 128 MiB of HBM per device.

v0:
```python
import jax
import jax.numpy as jnp
from jax import lax
from jax.sharding import Mesh
from jax.sharding import PartitionSpec as P

BROAD_CHANNEL_DIM = 128
THIN_CHANNEL_DIM = 64
GROUPS = 4
SP = ("sp_0", "sp_1")
SP_TP = ("sp_0", "sp_1", "tp")


rope_base = 10000.0
epsilon = 1e-06


def nothing_yet(value, identity):
    return jax.tree.map(
        lambda part, zero: jnp.zeros_like(part) + jnp.asarray(zero, part.dtype), value, identity
    )


def collected_together(value, axis):
    leaves = jax.tree.leaves(value)
    sequence = sorted(range(len(leaves)), key=lambda k: -leaves[k].size)
    width = (1, *leaves[sequence[0]].shape)[-1]
    lines = [
        jnp.pad(leaves[k].reshape(-1), (0, -leaves[k].size % width)).reshape(-1, width)
        for k in sequence
    ]
    both, at, found = (lax.all_gather(jnp.concatenate(lines), axis), 0, {})
    for k, line in zip(sequence, lines):
        slab = both[:, at : at + len(line)].reshape(len(both), -1)
        found[k] = slab[:, : leaves[k].size].reshape(-1, *leaves[k].shape)
        at += len(line)
    numbers = iter(range(len(leaves)))
    return jax.tree.map(lambda _: found[next(numbers)], value)


def prefix_by_axis(value, axes, combine, identity):
    before = start = nothing_yet(value, identity)
    total = value
    for axis in reversed(axes):
        count, here = (lax.axis_size(axis), lax.axis_index(axis))
        pieces = collected_together(
            jax.tree.map(
                lambda part, kind: part.astype(kind),
                total,
                (jnp.bfloat16, jnp.bfloat16, jnp.bfloat16, jnp.bfloat16),
            ),
            axis,
        )
        inside, total = (start, start)
        for k in range(count):
            passed = k < here
            total = combine(
                total, jax.tree.map(lambda part, own: part[k].astype(own.dtype), pieces, value)
            )
            inside = jax.tree.map(lambda new, old: jnp.where(passed, new, old), total, inside)
        before = combine(inside, before)
    return before


def rotate(payload_tensor, positions):
    channel_dimension = payload_tensor.shape[-1]
    half = channel_dimension // 2
    freq = rope_base ** (-jnp.arange(half, dtype=jnp.float32) * 2.0 / channel_dimension)
    angle = positions.astype(jnp.float32)[:, None, None] * freq[None, None, :]
    cosine = jnp.cos(angle)
    sine = jnp.sin(angle)
    first = payload_tensor[..., :half]
    second = payload_tensor[..., half:]
    return jnp.concatenate([first * cosine - second * sine, first * sine + second * cosine], -1)


def segment_terms(probe_tensor, lookup_tensor, payload_tensor, surge_forgetting, forgetting_speed):
    length = probe_tensor.shape[0]
    segment_tally = jnp.arange(length, dtype=jnp.float32)
    memory_matrix = (
        forgetting_speed[None, :] * segment_tally[:, None] + jnp.cumsum(surge_forgetting)[:, None]
    )
    causal = (segment_tally[:, None] >= segment_tally[None, :])[None]
    level_t = jnp.transpose(memory_matrix)
    gap = level_t[:, :, None] - level_t[:, None, :]
    decay = jnp.where(causal, jnp.exp(jnp.where(causal, gap, 0.0)), 0.0)
    attention_scores = jnp.einsum(
        "szr,yzr->zsy", probe_tensor, lookup_tensor, preferred_element_type=jnp.float32
    )
    weights = (attention_scores * decay).astype(jnp.bfloat16)
    inner = jnp.einsum("htm,mhe->the", weights, payload_tensor, preferred_element_type=jnp.float32)
    factor = jnp.exp(memory_matrix + forgetting_speed[None, :])
    tail = jnp.exp(memory_matrix[-1:, :] - memory_matrix)
    weighted_output = (lookup_tensor.astype(jnp.float32) * tail[:, :, None]).astype(jnp.bfloat16)
    state_update = jnp.einsum(
        "oup,our->upr", weighted_output, payload_tensor, preferred_element_type=jnp.float32
    )
    total = jnp.exp(memory_matrix[-1] + forgetting_speed)
    return (inner, factor, state_update, total)


def read_state(probe_tensor, state):
    return jnp.einsum("thd,hde->the", probe_tensor.astype(jnp.float32), state)


def keeping_multiplier(
    probe_source,
    lookup_tensor,
    payload_tensor,
    forgetting_speed,
    surge_forgetting,
    channel_dimension,
    segment_begin,
):
    length = probe_source.shape[0]
    heads = probe_source.shape[1] // channel_dimension
    places = segment_begin + jnp.arange(length, dtype=jnp.int32)
    spun_probe = rotate(
        probe_source.astype(jnp.float32).reshape(length, heads, channel_dimension), places
    ).astype(jnp.bfloat16)
    spun_lookup = (
        rotate(lookup_tensor.astype(jnp.float32).reshape(length, heads, channel_dimension), places)
        * channel_dimension ** (-0.5)
    ).astype(jnp.bfloat16)
    regrouped_payload = payload_tensor.reshape(length, heads, channel_dimension)
    block = min(512, length)
    count = length // block

    def divider_mark(array):
        return array.reshape((count, block) + array.shape[1:])

    def segment_walker(carry, piece):
        state, prefix = carry
        block_q, block_k, block_v, block_b = piece
        inner, factor, state_update, total = segment_terms(
            block_q, block_k, block_v, block_b, forgetting_speed
        )
        local = inner + factor[:, :, None] * read_state(block_q, state)
        return (
            (total[:, None, None] * state + state_update, prefix * total),
            (local, factor * prefix[None, :]),
        )

    opening_location = (
        jnp.zeros((heads, channel_dimension, channel_dimension), jnp.float32),
        jnp.ones((heads,), jnp.float32),
    )
    (state, decay), (local, reach) = lax.scan(
        segment_walker,
        opening_location,
        (
            divider_mark(spun_probe),
            divider_mark(spun_lookup),
            divider_mark(regrouped_payload),
            divider_mark(surge_forgetting),
        ),
    )
    return (
        spun_probe,
        local.reshape(length, heads, channel_dimension),
        reach.reshape(length, heads),
        decay,
        state,
    )


def finish(sublayer_final, emission_valve, scaling_coefficients):
    length, heads, channel_dimension = sublayer_final.shape
    normed = sublayer_final * lax.rsqrt(
        jnp.mean(sublayer_final * sublayer_final, -1, keepdims=True) + epsilon
    )
    gated = (
        normed.reshape(length, heads * channel_dimension)
        * scaling_coefficients[None, :]
        * jax.nn.silu(emission_valve.astype(jnp.float32))
    )
    return gated.astype(jnp.bfloat16)


def chain(earlier, later):
    return (
        earlier[0] * later[0],
        later[0][:, None, None] * earlier[1] + later[1],
        earlier[2] * later[2],
        later[2][:, None, None] * earlier[3] + later[3],
    )


def slot_positions(chosen, experts, cap):
    listed = chosen.reshape(-1)
    matches = (listed[:, None] == jnp.arange(experts, dtype=jnp.int32)[None, :]).astype(jnp.int32)
    before = jnp.cumsum(matches, 0) - matches
    order = jnp.sum(before * matches, 1)
    return (listed * cap + order).reshape(chosen.shape)


def fill_slots(rows_in, chosen, experts, cap):
    count = rows_in.shape[0]
    places = slot_positions(chosen, experts, cap).reshape(-1)
    owners = jnp.repeat(jnp.arange(count, dtype=jnp.int32), 2)
    source = jnp.full((experts * cap,), count, jnp.int32).at[places].set(owners)
    padded = jnp.concatenate([rows_in, jnp.zeros((1, rows_in.shape[1]), rows_in.dtype)], 0)
    return padded[source].reshape(experts, cap, rows_in.shape[1])


def on_device(
    broad_probe_tensor,
    broad_lookup_tensor,
    broad_payload_tensor,
    broad_emission_valve,
    slim_probe_tensor,
    slim_lookup_tensor,
    slim_payload_tensor,
    slim_emission_valve,
    broad_forgetting_speed,
    slim_forgetting_speed,
    broad_channel_scaling,
    slim_channel_scaling,
    surge_forgetting,
    broad_emission_proj,
    slim_emission_proj,
    skip_stream,
    premix_scaling_coeffs,
    routed_specialist_ids,
    routed_specialist_shares,
    specialist_valve_proj,
    specialist_expand_proj,
    specialist_contract_proj,
):
    length = broad_probe_tensor.shape[0]
    segment_begin = lax.axis_index(SP) * length
    wide_result = keeping_multiplier(
        broad_probe_tensor,
        broad_lookup_tensor,
        broad_payload_tensor,
        broad_forgetting_speed,
        surge_forgetting,
        BROAD_CHANNEL_DIM,
        segment_begin,
    )
    narrow_result = keeping_multiplier(
        slim_probe_tensor,
        slim_lookup_tensor,
        slim_payload_tensor,
        slim_forgetting_speed,
        surge_forgetting,
        THIN_CHANNEL_DIM,
        segment_begin,
    )
    identity = (
        jnp.ones_like(wide_result[3]),
        jnp.zeros_like(wide_result[4]),
        jnp.ones_like(narrow_result[3]),
        jnp.zeros_like(narrow_result[4]),
    )
    incoming = prefix_by_axis(
        (wide_result[3], wide_result[4], narrow_result[3], narrow_result[4]), SP, chain, identity
    )
    mixed_wide = finish(
        wide_result[1] + wide_result[2][:, :, None] * read_state(wide_result[0], incoming[1]),
        broad_emission_valve,
        broad_channel_scaling,
    )
    mixed_narrow = finish(
        narrow_result[1] + narrow_result[2][:, :, None] * read_state(narrow_result[0], incoming[3]),
        slim_emission_valve,
        slim_channel_scaling,
    )
    rows_wide, rows_narrow = (
        lax.all_to_all(mixed_wide, "tp", split_axis=0, concat_axis=1, tiled=True),
        lax.all_to_all(mixed_narrow, "tp", split_axis=0, concat_axis=1, tiled=True),
    )
    projected = jnp.dot(rows_wide, broad_emission_proj, preferred_element_type=jnp.float32)
    projected = projected + jnp.dot(
        rows_narrow, slim_emission_proj, preferred_element_type=jnp.float32
    )
    updated = skip_stream.astype(jnp.float32) + projected
    scale = lax.rsqrt(jnp.mean(updated * updated, -1, keepdims=True) + epsilon)
    normed = (updated * scale * premix_scaling_coeffs[None, :]).astype(jnp.bfloat16)
    rows = normed.shape[0]
    width = normed.shape[1]
    experts = lax.axis_size(SP) * specialist_valve_proj.shape[0]
    cap = rows * GROUPS // experts
    own_ids = lax.dynamic_slice_in_dim(routed_specialist_ids, lax.axis_index("tp") * rows, rows, 0)
    own_weights = lax.dynamic_slice_in_dim(
        routed_specialist_shares, lax.axis_index("tp") * rows, rows, 0
    )
    own_places = slot_positions(own_ids, experts, cap)
    sent = lax.all_to_all(
        fill_slots(normed, own_ids, experts, cap), SP, split_axis=0, concat_axis=0, tiled=True
    )
    arrived = lax.all_gather(sent, "tp", axis=0, tiled=True)
    slots = arrived.reshape(-1, width)
    emission_valve = jnp.dot(slots, specialist_valve_proj[0], preferred_element_type=jnp.float32)
    up = jnp.dot(slots, specialist_expand_proj[0], preferred_element_type=jnp.float32)
    hidden = (jax.nn.silu(emission_valve) * up).astype(jnp.bfloat16)
    summed = lax.psum_scatter(
        jnp.dot(hidden, specialist_contract_proj[0], preferred_element_type=jnp.float32).astype(
            jnp.bfloat16
        ),
        "tp",
        scatter_dimension=0,
        tiled=True,
    )
    expert_out = summed.reshape(experts, cap, width)
    returned = lax.all_to_all(expert_out, SP, split_axis=0, concat_axis=0, tiled=True)
    picked = returned.reshape(experts * cap, width)[own_places]
    mixture = jnp.sum(own_weights[:, :, None] * picked.astype(jnp.float32), 1)
    return (updated + mixture).astype(jnp.bfloat16)


def solution(mesh):
    finer = Mesh(mesh.devices.reshape(8, 4, mesh.shape["tp"]), ("sp_0", "sp_1", "tp"))
    return jax.shard_map(
        on_device,
        mesh=finer,
        in_specs=(
            P(SP, "tp"),
            P(SP, "tp"),
            P(SP, "tp"),
            P(SP, "tp"),
            P(SP, "tp"),
            P(SP, "tp"),
            P(SP, "tp"),
            P(SP, "tp"),
            P("tp"),
            P("tp"),
            P("tp"),
            P("tp"),
            P(SP),
            P(),
            P(),
            P(SP_TP, None),
            P(),
            P(SP, None),
            P(SP, None),
            P(SP, None, "tp"),
            P(SP, None, "tp"),
            P(SP, "tp", None),
        ),
        out_specs=P(SP_TP, None),
        check_vma=False,
    )
```

profile of v0, /device:TPU:1, one launch (start us, length us, event | category | flops | bytes accessed | tf_op | source)
XLA Modules:
  0.0 305.3 jit_solution(5164450144786927147)
XLA Ops:
  6.6 1.1 reduce-window.9
  7.9 0.7 multiply_add_fusion.2
  8.9 0.7 add_exponential_fusion
  9.6 0.7 broadcast_multiply_fusion.2
  10.3 1.0 copy.137
  11.4 1.0 copy.146
  12.4 1.0 copy.138
  16.1 1.3 fusion.80
  18.0 10.5 %all-gather.2 = bf16[4,194,128]{2,1,0:T(8,128)(2,1)S(1)} all-gather(bf16[1,194,128]{2,1,0:T(8,128)(2,1)S(1)} %maximum_bitcast_fusion), channel_id=2, replica_groups=mesh['sp_0'=8,'sp_1'=4,'tp'=8] {'sp_1'}, dimensions={0}, use_global_device_ids=true | all-gather | bytes 248320 | tf_op jit(solution)/shard_map/all_gather | solution.py:32
  33.2 23.0 %all-gather.3 = bf16[8,194,128]{2,1,0:T(8,128)(2,1)S(1)} all-gather(bf16[1,194,128]{2,1,0:T(8,128)(2,1)S(1)} %maximum_bitcast_fusion.1), channel_id=3, replica_groups=mesh['sp_0'=8,'sp_1'=4,'tp'=8] {'sp_0'}, dimensions={0}, use_global_device_ids=true | all-gather | bytes 446976 | tf_op jit(solution)/shard_map/all_gather | solution.py:32
  64.0 0.8 fusion.71
  64.8 13.8 %all-to-all-start = ((bf16[8,64,128]{2,1,0:T(8,128)(2,1)}), bf16[8,64,128]{2,1,0:T(8,128)(2,1)S(1)}, u32[]{:S(2)}, u32[]{:S(2)}) async-start(bf16[8,64,128]{2,1,0:T(8,128)(2,1)} %bitcast.66), calls=%async_computation | async-start | bytes 262144 | tf_op jit(solution)/shard_map/all_to_all | solution.py:270
  80.9 1.1 fusion.21
  82.7 0.8 constant_dynamic-slice_fusion
  84.6 1.0 scatter_custom_fusion
  85.6 0.7 fusion.70
  86.4 4.8 %all-to-all-start.1 = ((bf16[8,64,128]{2,1,0:T(8,128)(2,1)}), bf16[8,64,128]{2,1,0:T(8,128)(2,1)S(1)}, u32[]{:S(2)}, u32[]{:S(2)}) async-start(bf16[8,64,128]{2,1,0:T(8,128)(2,1)} %bitcast.82), calls=%async_computation.1 | async-start | bytes 262144 | tf_op jit(solution)/shard_map/all_to_all | solution.py:271
  91.2 3.1 %fusion.74 = f32[64,2048]{1,0:T(8,128)S(1)} fusion(bf16[1024,2048]{1,0:T(8,128)(2,1)} %param.35, bf16[8,64,128]{2,1,0:T(8,128)(2,1)S(1)} %all-to-all-done), kind=kOutput, calls=%fused_computation.98 | convolution fusion | flops 268435456 | bytes 4849664 | tf_op jit(solution)/shard_map/dot_general | solution.py:273
  94.3 2.1 all-to-all-done.1
  96.5 3.2 %multiply_reduce_fusion.1 = (f32[64]{0:T(128)S(1)}, f32[64,2048]{1,0:T(8,128)S(1)}) fusion(f32[64,2048]{1,0:T(8,128)S(1)} %fusion.74, bf16[1024,2048]{1,0:T(8,128)(2,1)} %param.36, bf16[64,2048]{1,0:T(8,128)(2,1)S(1)} %copy-done.1, bf16[8,64,128]{2,1,0:T(8,128)(2,1)S(1)} %all-to-all-done.1), kind=kOutput, calls=%fused_computation.51 | convolution fusion | flops 269090752 | bytes 5636352 | tf_op jit(solution)/shard_map/dot_general | solution.py:274
  99.8 1.4 gather_fusion
  101.2 32.8 %all_to_all.48 = bf16[32,8,2048]{2,1,0:T(8,128)(2,1)} all-to-all(bf16[32,8,2048]{2,1,0:T(8,128)(2,1)S(1)} %bitcast.268), channel_id=1, replica_groups=mesh['sp_0'=8,'sp_1'=4,'tp'=8] {'sp_0','sp_1'}, dimensions={0} | all-to-all | bytes 2097152 | tf_op jit(solution)/shard_map/all_to_all | solution.py:289
  134.3 50.0 %all-gather.6.cloned.1.call-done = bf16[256,8,2048]{2,1,0:T(8,128)(2,1)} async-done(((bf16[32,8,2048]{2,1,0:T(8,128)(2,1)}), bf16[256,8,2048]{2,1,0:T(8,128)(2,1)}) %all-gather.6.cloned.1.call-update) | async-done | bytes 8388624 | tf_op jit(solution)/shard_map/all_gather | solution.py:292
  184.3 7.3 %fusion.2 = f32[2048,256]{1,0:T(8,128)} fusion(bf16[256,8,2048]{2,1,0:T(8,128)(2,1)} %all-gather.6.cloned.1.call-done, bf16[1,2048,256]{2,1,0:T(8,128)(2,1)} %param.41), kind=kOutput, calls=%fused_computation.5 | convolution fusion | flops 2147483648 | bytes 11534336 | tf_op jit(solution)/shard_map/dot_general | solution.py:294
  191.6 13.1 %convolution_convert_fusion = bf16[2048,2048]{1,0:T(8,128)(2,1)} fusion(bf16[256,8,2048]{2,1,0:T(8,128)(2,1)} %all-gather.6.cloned.1.call-done, f32[2048,256]{1,0:T(8,128)} %fusion.2, bf16[1,256,2048]{2,1,0:T(8,128)(2,1)S(1)} %copy-done, bf16[1,2048,256]{2,1,0:T(8,128)(2,1)S(1)} %copy-done.10), kind=kOutput, calls=%fused_computation.7 | convolution fusion | flops 4302307328 | bytes 20971520 | tf_op jit(solution)/shard_map/dot_general | solution.py:298
  204.7 54.4 %reduce-scatter.2.cloned.1.call-done = bf16[256,2048]{1,0:T(8,128)(2,1)} async-done(((bf16[2048,2048]{1,0:T(8,128)(2,1)}), bf16[256,2048]{1,0:T(8,128)(2,1)}) %reduce-scatter.2.cloned.1.call-update) | async-done | bytes 1048592 | tf_op jit(solution)/shard_map/reduce_scatter | solution.py:297
  259.1 9.5 %all-to-all-start.3 = ((bf16[32,8,2048]{2,1,0:T(8,128)(2,1)}), bf16[32,8,2048]{2,1,0:T(8,128)(2,1)S(1)}, u32[]{:S(2)}, u32[]{:S(2)}) async-start(bf16[32,8,2048]{2,1,0:T(8,128)(2,1)} %bitcast.269), calls=%async_computation.4 | async-start | bytes 2097152 | tf_op jit(solution)/shard_map/all_to_all | solution.py:306
  268.8 0.8 constant_dynamic-slice_fusion.1
  269.6 24.9 %all-to-all-done.3 = bf16[32,8,2048]{2,1,0:T(8,128)(2,1)S(1)} async-done(((bf16[32,8,2048]{2,1,0:T(8,128)(2,1)}), bf16[32,8,2048]{2,1,0:T(8,128)(2,1)S(1)}, u32[]{:S(2)}, u32[]{:S(2)}) %all-to-all-start.3) | async-done | bytes 1048608 | tf_op jit(solution)/shard_map/all_to_all | solution.py:306
  294.5 0.9 gather_fusion.1
  296.1 1.5 multiply_reduce_fusion
  297.7 0.8 add_convert_fusion
  (133 shorter events, 11.1 us)
Async XLA Ops:
  6.5 185.0 %copy-start = (bf16[1,256,2048]{2,1,0:T(8,128)(2,1)S(1)}, bf16[1,256,2048]{2,1,0:T(8,128)(2,1)}, u32[]{:S(2)}) copy-start(bf16[1,256,2048]{2,1,0:T(8,128)(2,1)} %param.43) | copy-start | bytes 3145732
  6.5 9.5 %copy-start.5 = (bf16[512,128]{1,0:T(8,128)(2,1)S(1)}, bf16[512,128]{1,0:T(8,128)(2,1)}, u32[]{:S(2)}) copy-start(bf16[512,128]{1,0:T(8,128)(2,1)} %param.22) | copy-start | bytes 393220
  6.5 9.5 %copy-start.4 = (bf16[512,128]{1,0:T(8,128)(2,1)S(1)}, bf16[512,128]{1,0:T(8,128)(2,1)}, u32[]{:S(2)}) copy-start(bf16[512,128]{1,0:T(8,128)(2,1)} %param.23) | copy-start | bytes 393220
  13.8 3.8 %copy-start.11 = (bf16[512,128]{1,0:T(8,128)(2,1)S(1)}, bf16[512,128]{1,0:T(8,128)(2,1)}, u32[]{:S(2)}) copy-start(bf16[512,128]{1,0:T(8,128)(2,1)} %param.24) | copy-start | bytes 393220
  62.6 1.3 copy-start.2
  62.6 1.3 copy-start.8
  63.2 15.4 %copy-start.7 = (f32[2]{0:T(128)S(1)}, f32[2]{0:T(128)}, u32[]{:S(2)}) copy-start(f32[2]{0:T(128)} %param.31) | copy-start | bytes 28
  64.8 21.6 %all-to-all-start = ((bf16[8,64,128]{2,1,0:T(8,128)(2,1)}), bf16[8,64,128]{2,1,0:T(8,128)(2,1)S(1)}, u32[]{:S(2)}, u32[]{:S(2)}) async-start(bf16[8,64,128]{2,1,0:T(8,128)(2,1)} %bitcast.66), calls=%async_computation | async-start | bytes 262144 | tf_op jit(solution)/shard_map/all_to_all | solution.py:270
  82.0 3.6 %copy-start.3 = (bf16[512,128]{1,0:T(8,128)(2,1)S(1)}, bf16[512,128]{1,0:T(8,128)(2,1)}, u32[]{:S(2)}) copy-start(bf16[512,128]{1,0:T(8,128)(2,1)} %param.29) | copy-start | bytes 393220
  82.0 3.6 %copy-start.9 = (f32[128]{0:T(128)S(1)}, f32[128]{0:T(128)}, u32[]{:S(2)}) copy-start(f32[128]{0:T(128)} %param.33) | copy-start | bytes 1540
  86.4 10.1 %all-to-all-start.1 = ((bf16[8,64,128]{2,1,0:T(8,128)(2,1)}), bf16[8,64,128]{2,1,0:T(8,128)(2,1)S(1)}, u32[]{:S(2)}, u32[]{:S(2)}) async-start(bf16[8,64,128]{2,1,0:T(8,128)(2,1)} %bitcast.82), calls=%async_computation.1 | async-start | bytes 262144 | tf_op jit(solution)/shard_map/all_to_all | solution.py:271
  91.2 5.2 %copy-start.1 = (bf16[64,2048]{1,0:T(8,128)(2,1)S(1)}, bf16[64,2048]{1,0:T(8,128)(2,1)}, u32[]{:S(2)}) copy-start(bf16[64,2048]{1,0:T(8,128)(2,1)} %param.37) | copy-start | bytes 786436
  91.2 93.0 %all-gather.6.cloned.1.call-start = ((), (), s32[]{:S(2)}) async-start(), calls=%async_computation.5 | async-start | bytes 9437184 | tf_op jit(solution)/shard_map/all_gather | solution.py:292
  94.3 5.4 %copy-start.6 = (f32[2048]{0:T(1024)S(1)}, f32[2048]{0:T(1024)}, u32[]{:S(2)}) copy-start(f32[2048]{0:T(1024)} %param.38) | copy-start | bytes 24580
  134.0 57.5 %copy-start.10 = (bf16[1,2048,256]{2,1,0:T(8,128)(2,1)S(1)}, bf16[1,2048,256]{2,1,0:T(8,128)(2,1)}, u32[]{:S(2)}) copy-start(bf16[1,2048,256]{2,1,0:T(8,128)(2,1)} %param.42) | copy-start | bytes 3145732
  134.1 125.1 %reduce-scatter.2.cloned.1.call-start = ((), (), s32[]{:S(2)}) async-start(), calls=%async_computation.6 | async-start | bytes 9437184 | tf_op jit(solution)/shard_map/reduce_scatter | solution.py:297
  259.1 35.4 %all-to-all-start.3 = ((bf16[32,8,2048]{2,1,0:T(8,128)(2,1)}), bf16[32,8,2048]{2,1,0:T(8,128)(2,1)S(1)}, u32[]{:S(2)}, u32[]{:S(2)}) async-start(bf16[32,8,2048]{2,1,0:T(8,128)(2,1)} %bitcast.269), calls=%async_computation.4 | async-start | bytes 2097152 | tf_op jit(solution)/shard_map/all_to_all | solution.py:306
Sparse Core Ops, SparseCore 0:
  134.2 50.0 all-gather.5
  204.8 54.2 reduce-scatter.1
where the time goes:
time: 308 us; the launch traced here: 305 us
  waiting for transfers between devices  131 us (43%)
  blocking collectives  66.3 us (22%)
  matrix products  30.1 us (10%)
  starting transfers between devices  28.3 us (9%)
  between operations  24.4 us (8%)
  local copies, waits for them, and re-layouts  14.4 us (5%)
  other arithmetic  10.2 us (3%)
    reduce_scatter x1, waiting for transfers between devices, on_device(): lax.psum_scatter(jnp.dot(hidden, specialist_contract_proj[0], preferred_e...  54.4 us
    all_gather x1, waiting for transfers between devices, on_device(): arrived = lax.all_gather(sent, 'tp', axis=0, tiled=True)  50 us
    all_gather x2, blocking collectives, collected_together(): both, at, found = (lax.all_gather(jnp.concatenate(lines), axis), 0, {})  33.5 us
    all_to_all x1, blocking collectives, on_device(): lax.all_to_all(fill_slots(normed, own_ids, experts, cap), SP, split_axis=...  32.8 us
    all_to_all x1, waiting for transfers between devices, on_device(): lax.all_to_all(expert_out, SP, split_axis=0, concat_axis=0, tiled=True)  24.9 us
    all_to_all x1, starting transfers between devices, on_device(): lax.all_to_all(mixed_wide, 'tp', split_axis=0, concat_axis=1, tiled=True)  13.8 us
    dot_general x1, matrix products, on_device(): jnp.dot(hidden, specialist_contract_proj[0], preferred_element_type=jnp.f...  13.1 us
    all_to_all x1, starting transfers between devices, on_device(): lax.all_to_all(expert_out, SP, split_axis=0, concat_axis=0, tiled=True)  9.54 us
  transfers between devices with their start and end apart: 5, of which 4 were waited for; matrix products, arithmetic and copies ran while one was open for 4% of the time, Pallas kernels for 0%

commit v1 on v0

--- a/solution.py
+++ b/solution.py
@@ -229,6 +229,9 @@
 ):
     length = broad_probe_tensor.shape[0]
     segment_begin = lax.axis_index(SP) * length
+    valve_all = lax.all_gather(specialist_valve_proj[0], "tp")
+    expand_all = lax.all_gather(specialist_expand_proj[0], "tp")
+    contract_all = lax.all_gather(specialist_contract_proj[0], "tp")
     wide_result = keeping_multiplier(
         broad_probe_tensor,
         broad_lookup_tensor,
@@ -289,19 +292,13 @@
     sent = lax.all_to_all(
         fill_slots(normed, own_ids, experts, cap), SP, split_axis=0, concat_axis=0, tiled=True
     )
-    arrived = lax.all_gather(sent, "tp", axis=0, tiled=True)
-    slots = arrived.reshape(-1, width)
-    emission_valve = jnp.dot(slots, specialist_valve_proj[0], preferred_element_type=jnp.float32)
-    up = jnp.dot(slots, specialist_expand_proj[0], preferred_element_type=jnp.float32)
-    hidden = (jax.nn.silu(emission_valve) * up).astype(jnp.bfloat16)
-    summed = lax.psum_scatter(
-        jnp.dot(hidden, specialist_contract_proj[0], preferred_element_type=jnp.float32).astype(
-            jnp.bfloat16
-        ),
-        "tp",
-        scatter_dimension=0,
-        tiled=True,
-    )
+    slots = sent.reshape(-1, width)
+    emission_valve = jnp.einsum("sd,tdf->stf", slots, valve_all, preferred_element_type=jnp.float32)
+    up = jnp.einsum("sd,tdf->stf", slots, expand_all, preferred_element_type=jnp.float32)
+    hidden = (jax.nn.silu(emission_valve) * up).astype(jnp.bfloat16).reshape(slots.shape[0], -1)
+    summed = jnp.dot(
+        hidden, contract_all.reshape(-1, width), preferred_element_type=jnp.float32
+    ).astype(jnp.bfloat16)
     expert_out = summed.reshape(experts, cap, width)
     returned = lax.all_to_all(expert_out, SP, split_axis=0, concat_axis=0, tiled=True)
     picked = returned.reshape(experts * cap, width)[own_places]

time: 308 us -> 236 us (0.77)
  waiting for transfers between devices: 131 us -> 67.9 us
    reduce_scatter x1 -> x0, waiting for transfers between devices: 54.4 us -> none  [on_device(): lax.psum_scatter(jnp.dot(hidden, specialist_contract_proj[0], preferred_e...]
    all_gather x1 -> x3, waiting for transfers between devices: 50 us -> 36 us  [the longest x1 36 us: on_device(): valve_all = lax.all_gather(specialist_valve_proj[0], 'tp')]
  transfers between devices with their start and end apart: 5 -> 6, of which waited for: 4 -> 3; matrix products, arithmetic and copies ran while one was open for 4% -> 14% of each run, Pallas kernels for 0% -> 0%
where the time goes in v1:
time: 236 us; the launch traced here: 235 us
  blocking collectives  68.5 us (29%)
  waiting for transfers between devices  67.9 us (29%)
  matrix products  29.2 us (12%)
  starting transfers between devices  25.9 us (11%)
  between operations  23.9 us (10%)
  local copies, waits for them, and re-layouts  11.7 us (5%)
  other arithmetic  7.51 us (3%)
    all_gather x1, waiting for transfers between devices, on_device(): valve_all = lax.all_gather(specialist_valve_proj[0], 'tp')  36 us
    all_gather x2, blocking collectives, collected_together(): both, at, found = (lax.all_gather(jnp.concatenate(lines), axis), 0, {})  35.8 us
    all_to_all x1, blocking collectives, on_device(): lax.all_to_all(fill_slots(normed, own_ids, experts, cap), SP, split_axis=...  32.7 us
    all_to_all x1, waiting for transfers between devices, on_device(): lax.all_to_all(expert_out, SP, split_axis=0, concat_axis=0, tiled=True)  25.9 us
    dot_general x1, matrix products, on_device(): jnp.dot(hidden, contract_all.reshape(-1, width), preferred_element_type=j...  11.9 us
    all_to_all x1, starting transfers between devices, on_device(): lax.all_to_all(mixed_wide, 'tp', split_axis=0, concat_axis=1, tiled=True)  11.5 us
    all_to_all x1, starting transfers between devices, on_device(): lax.all_to_all(expert_out, SP, split_axis=0, concat_axis=0, tiled=True)  9.54 us
    dot_general x1, matrix products, on_device(): jnp.einsum('sd,tdf->stf', slots, expand_all, preferred_element_type=jnp.f...  7.47 us
  transfers between devices with their start and end apart: 6, of which 3 were waited for; matrix products, arithmetic and copies ran while one was open for 14% of the time, Pallas kernels for 0%

profile of v1, /device:TPU:1, one launch (start us, length us, event | category | flops | bytes accessed | tf_op | source)
XLA Modules:
  0.0 234.6 jit_solution(13604464351282056884)
XLA Ops:
  6.6 0.7 all-gather.10.cloned.1.call-update
  7.3 0.7 all-gather.12.cloned.1.call-update
  8.1 0.7 all-gather.8.cloned.1.call-update
  10.9 0.6 slice.349
  12.9 1.3 fusion.70
  14.8 10.5 %all-gather.2 = bf16[4,194,128]{2,1,0:T(8,128)(2,1)S(1)} all-gather(bf16[1,194,128]{2,1,0:T(8,128)(2,1)S(1)} %maximum_bitcast_fusion), channel_id=2, replica_groups=mesh['sp_0'=8,'sp_1'=4,'tp'=8] {'sp_1'}, dimensions={0}, use_global_device_ids=true | all-gather | bytes 248320 | tf_op jit(solution)/shard_map/all_gather | solution.py:32
  25.3 0.6 fusion.248
  29.9 25.3 %all-gather.3 = bf16[8,194,128]{2,1,0:T(8,128)(2,1)S(1)} all-gather(bf16[1,194,128]{2,1,0:T(8,128)(2,1)S(1)} %maximum_bitcast_fusion.1), channel_id=3, replica_groups=mesh['sp_0'=8,'sp_1'=4,'tp'=8] {'sp_0'}, dimensions={0}, use_global_device_ids=true | all-gather | bytes 446976 | tf_op jit(solution)/shard_map/all_gather | solution.py:32
  55.2 0.6 fusion.247
  61.4 0.6 fusion.10
  62.7 0.8 fusion.61
  63.5 11.5 %all-to-all-start = ((bf16[8,64,128]{2,1,0:T(8,128)(2,1)}), bf16[8,64,128]{2,1,0:T(8,128)(2,1)S(1)}, u32[]{:S(2)}, u32[]{:S(2)}) async-start(bf16[8,64,128]{2,1,0:T(8,128)(2,1)} %bitcast.66), calls=%async_computation | async-start | bytes 262144 | tf_op jit(solution)/shard_map/all_to_all | solution.py:273
  77.4 1.1 fusion.11
  79.2 0.8 constant_dynamic-slice_fusion
  81.1 1.0 scatter_custom_fusion
  82.1 0.7 fusion.60
  82.9 4.8 %all-to-all-start.1 = ((bf16[8,64,128]{2,1,0:T(8,128)(2,1)}), bf16[8,64,128]{2,1,0:T(8,128)(2,1)S(1)}, u32[]{:S(2)}, u32[]{:S(2)}) async-start(bf16[8,64,128]{2,1,0:T(8,128)(2,1)} %bitcast.82), calls=%async_computation.1 | async-start | bytes 262144 | tf_op jit(solution)/shard_map/all_to_all | solution.py:274
  87.7 3.1 %fusion.64 = f32[64,2048]{1,0:T(8,128)S(1)} fusion(bf16[1024,2048]{1,0:T(8,128)(2,1)} %param.35, bf16[8,64,128]{2,1,0:T(8,128)(2,1)S(1)} %all-to-all-done), kind=kOutput, calls=%fused_computation.94 | convolution fusion | flops 268435456 | bytes 4849664 | tf_op jit(solution)/shard_map/dot_general | solution.py:276
  90.9 3.9 %all-to-all-done.1 = bf16[8,64,128]{2,1,0:T(8,128)(2,1)S(1)} async-done(((bf16[8,64,128]{2,1,0:T(8,128)(2,1)}), bf16[8,64,128]{2,1,0:T(8,128)(2,1)S(1)}, u32[]{:S(2)}, u32[]{:S(2)}) %all-to-all-start.1) | async-done | bytes 131104 | tf_op jit(solution)/shard_map/all_to_all | solution.py:274
  94.8 3.2 %multiply_reduce_fusion.1 = (f32[64]{0:T(128)S(1)}, f32[64,2048]{1,0:T(8,128)S(1)}) fusion(f32[64,2048]{1,0:T(8,128)S(1)} %fusion.64, bf16[1024,2048]{1,0:T(8,128)(2,1)} %param.36, bf16[64,2048]{1,0:T(8,128)(2,1)S(1)} %copy-done.1, bf16[8,64,128]{2,1,0:T(8,128)(2,1)S(1)} %all-to-all-done.1), kind=kOutput, calls=%fused_computation.47 | convolution fusion | flops 269090752 | bytes 5636352 | tf_op jit(solution)/shard_map/dot_general | solution.py:277
  98.2 1.4 gather_fusion
  99.6 32.7 %all_to_all.48 = bf16[32,8,2048]{2,1,0:T(8,128)(2,1)S(1)} all-to-all(bf16[32,8,2048]{2,1,0:T(8,128)(2,1)S(1)} %bitcast.266), channel_id=1, replica_groups=mesh['sp_0'=8,'sp_1'=4,'tp'=8] {'sp_0','sp_1'}, dimensions={0} | all-to-all | bytes 2097152 | tf_op jit(solution)/shard_map/all_to_all | solution.py:292
  132.3 7.5 %fusion.18 = f32[256,8,256]{2,0,1:T(8,128)} fusion(bf16[8,2048,256]{2,1,0:T(8,128)(2,1)} %all-gather.10.cloned.1.call-done, bf16[32,8,2048]{2,1,0:T(8,128)(2,1)S(1)} %all_to_all.48), kind=kOutput, calls=%fused_computation.32 | convolution fusion | flops 2147483648 | bytes 11534336 | tf_op jit(solution)/shard_map/sd,tdf->stf/dot_general | solution.py:297
  139.7 36.0 %all-gather.8.cloned.1.call-done = bf16[8,2048,256]{2,1,0:T(8,128)(2,1)} async-done(((bf16[1,2048,256]{2,1,0:T(8,128)(2,1)}), bf16[8,2048,256]{2,1,0:T(8,128)(2,1)}) %all-gather.8.cloned.1.call-update) | async-done | bytes 8388624 | tf_op jit(solution)/shard_map/all_gather | solution.py:232
  175.8 11.9 %fusion.1 = bf16[32,8,2048]{2,1,0:T(8,128)(2,1)} fusion(bf16[8,256,2048]{2,1,0:T(8,128)(2,1)} %all-gather.12.cloned.1.call-done, f32[256,8,256]{2,0,1:T(8,128)} %fusion.18, bf16[8,2048,256]{2,1,0:T(8,128)(2,1)} %all-gather.8.cloned.1.call-done, bf16[32,8,2048]{2,1,0:T(8,128)(2,1)S(1)} %all_to_all.48), kind=kOutput, calls=%fused_computation.5 | convolution fusion | flops 4298637312 | bytes 20971520 | tf_op jit(solution)/shard_map/dot_general | solution.py:299
  187.7 9.5 %all-to-all-start.3 = ((bf16[32,8,2048]{2,1,0:T(8,128)(2,1)}), bf16[32,8,2048]{2,1,0:T(8,128)(2,1)S(1)}, u32[]{:S(2)}, u32[]{:S(2)}) async-start(bf16[32,8,2048]{2,1,0:T(8,128)(2,1)} %fusion.1), calls=%async_computation.3 | async-start | bytes 2097152 | tf_op jit(solution)/shard_map/all_to_all | solution.py:303
  197.4 0.8 constant_dynamic-slice_fusion.1
  198.3 25.9 %all-to-all-done.3 = bf16[32,8,2048]{2,1,0:T(8,128)(2,1)S(1)} async-done(((bf16[32,8,2048]{2,1,0:T(8,128)(2,1)}), bf16[32,8,2048]{2,1,0:T(8,128)(2,1)S(1)}, u32[]{:S(2)}, u32[]{:S(2)}) %all-to-all-start.3) | async-done | bytes 1048608 | tf_op jit(solution)/shard_map/all_to_all | solution.py:303
  224.2 0.9 gather_fusion.1
  225.1 0.7 reshape.1207
  225.8 1.6 multiply_reduce_fusion
  227.3 0.8 add_convert_fusion
  (140 shorter events, 8.6 us)
Async XLA Ops:
  6.5 7.8 %copy-start = (bf16[512,128]{1,0:T(8,128)(2,1)S(1)}, bf16[512,128]{1,0:T(8,128)(2,1)}, u32[]{:S(2)}) copy-start(bf16[512,128]{1,0:T(8,128)(2,1)} %param.24) | copy-start | bytes 393220
  6.5 2.3 copy-start.11
  6.5 2.9 %copy-start.10 = (f32[2]{0:T(128)S(1)}, f32[2]{0:T(128)}, u32[]{:S(2)}) copy-start(f32[2]{0:T(128)} %param.31) | copy-start | bytes 28
  6.5 3.0 %copy-start.2 = (bf16[512,128]{1,0:T(8,128)(2,1)S(1)}, bf16[512,128]{1,0:T(8,128)(2,1)}, u32[]{:S(2)}) copy-start(bf16[512,128]{1,0:T(8,128)(2,1)} %param.27) | copy-start | bytes 393220
  6.5 3.1 %copy-start.3 = (bf16[512,128]{1,0:T(8,128)(2,1)S(1)}, bf16[512,128]{1,0:T(8,128)(2,1)}, u32[]{:S(2)}) copy-start(bf16[512,128]{1,0:T(8,128)(2,1)} %param.26) | copy-start | bytes 393220
  6.5 3.2 %copy-start.6 = (bf16[512,128]{1,0:T(8,128)(2,1)S(1)}, bf16[512,128]{1,0:T(8,128)(2,1)}, u32[]{:S(2)}) copy-start(bf16[512,128]{1,0:T(8,128)(2,1)} %param.28) | copy-start | bytes 393220
  6.6 125.7 %all-gather.10.cloned.1.call-start = ((), (), s32[]{:S(2)}) async-start(), calls=%async_computation.5 | async-start | bytes 9437184 | tf_op jit(solution)/shard_map/all_gather | solution.py:233
  7.3 132.5 %all-gather.12.cloned.1.call-start = ((), (), s32[]{:S(2)}) async-start(), calls=%async_computation.6 | async-start | bytes 9437184 | tf_op jit(solution)/shard_map/all_gather | solution.py:234
  8.0 4.8 %copy-start.7 = (bf16[512,128]{1,0:T(8,128)(2,1)S(1)}, bf16[512,128]{1,0:T(8,128)(2,1)}, u32[]{:S(2)}) copy-start(bf16[512,128]{1,0:T(8,128)(2,1)} %param.23) | copy-start | bytes 393220
  8.1 4.8 %copy-start.8 = (bf16[512,128]{1,0:T(8,128)(2,1)S(1)}, bf16[512,128]{1,0:T(8,128)(2,1)}, u32[]{:S(2)}) copy-start(bf16[512,128]{1,0:T(8,128)(2,1)} %param.22) | copy-start | bytes 393220
  8.1 167.7 %all-gather.8.cloned.1.call-start = ((), (), s32[]{:S(2)}) async-start(), calls=%async_computation.4 | async-start | bytes 9437184 | tf_op jit(solution)/shard_map/all_gather | solution.py:232
  61.4 1.3 copy-start.4
  61.4 1.3 copy-start.12
  63.5 19.4 %all-to-all-start = ((bf16[8,64,128]{2,1,0:T(8,128)(2,1)}), bf16[8,64,128]{2,1,0:T(8,128)(2,1)S(1)}, u32[]{:S(2)}, u32[]{:S(2)}) async-start(bf16[8,64,128]{2,1,0:T(8,128)(2,1)} %bitcast.66), calls=%async_computation | async-start | bytes 262144 | tf_op jit(solution)/shard_map/all_to_all | solution.py:273
  78.5 3.6 %copy-start.5 = (bf16[512,128]{1,0:T(8,128)(2,1)S(1)}, bf16[512,128]{1,0:T(8,128)(2,1)}, u32[]{:S(2)}) copy-start(bf16[512,128]{1,0:T(8,128)(2,1)} %param.29) | copy-start | bytes 393220
  78.5 3.6 %copy-start.13 = (f32[128]{0:T(128)S(1)}, f32[128]{0:T(128)}, u32[]{:S(2)}) copy-start(f32[128]{0:T(128)} %param.33) | copy-start | bytes 1540
  82.9 11.9 %all-to-all-start.1 = ((bf16[8,64,128]{2,1,0:T(8,128)(2,1)}), bf16[8,64,128]{2,1,0:T(8,128)(2,1)S(1)}, u32[]{:S(2)}, u32[]{:S(2)}) async-start(bf16[8,64,128]{2,1,0:T(8,128)(2,1)} %bitcast.82), calls=%async_computation.1 | async-start | bytes 262144 | tf_op jit(solution)/shard_map/all_to_all | solution.py:274
  87.7 7.1 %copy-start.1 = (bf16[64,2048]{1,0:T(8,128)(2,1)S(1)}, bf16[64,2048]{1,0:T(8,128)(2,1)}, u32[]{:S(2)}) copy-start(bf16[64,2048]{1,0:T(8,128)(2,1)} %param.37) | copy-start | bytes 786436
  90.9 7.2 %copy-start.9 = (f32[2048]{0:T(1024)S(1)}, f32[2048]{0:T(1024)}, u32[]{:S(2)}) copy-start(f32[2048]{0:T(1024)} %param.38) | copy-start | bytes 24580
  187.7 36.4 %all-to-all-start.3 = ((bf16[32,8,2048]{2,1,0:T(8,128)(2,1)}), bf16[32,8,2048]{2,1,0:T(8,128)(2,1)S(1)}, u32[]{:S(2)}, u32[]{:S(2)}) async-start(bf16[32,8,2048]{2,1,0:T(8,128)(2,1)} %fusion.1), calls=%async_computation.3 | async-start | bytes 2097152 | tf_op jit(solution)/shard_map/all_to_all | solution.py:303
Sparse Core Ops, SparseCore 0:
  9.2 56.4 all-gather.9
  67.6 53.8 all-gather.11
  123.3 52.4 all-gather.7
